TPU v7x, 32 devices: a whole 2x2x4 slice. The times are simulated.
32 devices in a mesh: rep: 2 (over y), fs: 4 (over z), tp: 4 (over x, core).
Axes of the slice: x: 2, y: 2, z: 4, core: 2. Of those that a mesh axis runs over, the one named last changes fastest.
Arguments:
- stream: bfloat16 [2048, 1536], P(('rep', 'fs')), may hold values from -6 to 6
- mix_pre_gain: float32 [1536], replicated, may hold values from 0.1 to 1.9
- w_outer_gate: bfloat16 [1536, 768], P('fs', 'tp'), may hold values from -0.15625 to 0.15625
- w_inner_gate: bfloat16 [1536, 768], P('fs', 'tp'), may hold values from -0.15625 to 0.15625
- w_value: bfloat16 [1536, 768], P('fs', 'tp'), may hold values from -0.15625 to 0.15625
- mix_taps: float32 [3, 768], P(None, 'tp'), may hold values from -3 to 3
- w_mix_out: bfloat16 [768, 1536], P('tp', 'fs'), may hold values from -0.3125 to 0.3125
- mix_post_gain: float32 [1536], replicated, may hold values from 0.1 to 1.9
- ffn_pre_gain: float32 [1536], replicated, may hold values from 0.1 to 1.9
- w_linear: bfloat16 [1536, 4224], P('fs', 'tp'), may hold values from -0.15625 to 0.15625
- w_gated: bfloat16 [1536, 4224], P('fs', 'tp'), may hold values from -0.15625 to 0.15625
- ffn_taps: float32 [3, 4224], P(None, 'tp'), may hold values from -3 to 3
- ffn_bias: float32 [4224], P('tp'), may hold values from -3 to 3
- w_down: bfloat16 [4224, 1536], P('tp', 'fs'), may hold values from -0.125 to 0.125
- ffn_post_gain: float32 [1536], replicated, may hold values from 0.1 to 1.9
Outputs:
- result: bfloat16 [2048, 1536], P(('rep', 'fs'))
All inputs are finite; a program needn't handle non-finite values.
Results may differ from a plain program's by a relative error of at most 0.023.
Values may be sent and summed in bfloat16 or wider, within the bound.
A program may use at most 64 MiB of HBM per device.

v0:
```python
import jax
import jax.numpy as jnp
from jax import lax
from jax.sharding import PartitionSpec as P

SEQ_LEN = 128
EPS = 1e-06


def norm_scale(values, gain):
    return values * lax.rsqrt(jnp.mean(values * values, axis=-1, keepdims=True) + EPS) * gain


def conv_three(values, taps):
    height, breadth = values.shape
    grouped = values.reshape(height // SEQ_LEN, SEQ_LEN, breadth)
    padded = jnp.pad(grouped, ((0, 0), (1, 1), (0, 0)))
    mixed = taps[0] * padded[:, :-2] + taps[1] * padded[:, 1:-1] + taps[2] * padded[:, 2:]
    return mixed.reshape(height, breadth)


def settle(partial_value, resid, post_gain):
    branch = lax.psum(partial_value.astype(jnp.bfloat16), "tp")
    return (resid + norm_scale(branch.astype(jnp.float32), post_gain)).astype(jnp.bfloat16)


def on_device(
    stream,
    mix_pre_gain,
    w_outer_gate,
    w_inner_gate,
    w_value,
    mix_taps,
    w_mix_out,
    mix_post_gain,
    ffn_pre_gain,
    w_linear,
    w_gated,
    ffn_taps,
    ffn_bias,
    w_down,
    ffn_post_gain,
):
    resid = stream.astype(jnp.float32)
    normed = norm_scale(resid, mix_pre_gain).astype(jnp.bfloat16)
    full_outer, full_inner, full_value = (
        lax.all_gather(w_outer_gate, "fs", axis=0, tiled=True),
        lax.all_gather(w_inner_gate, "fs", axis=0, tiled=True),
        lax.all_gather(w_value, "fs", axis=0, tiled=True),
    )
    outer = jnp.dot(normed, full_outer, preferred_element_type=jnp.float32)
    inner = jnp.dot(normed, full_inner, preferred_element_type=jnp.float32)
    value = jnp.dot(normed, full_value, preferred_element_type=jnp.float32)
    outer = outer.astype(jnp.bfloat16)
    inner = inner.astype(jnp.bfloat16)
    value = value.astype(jnp.bfloat16)
    product = inner.astype(jnp.float32) * value.astype(jnp.float32)
    mixed = (outer.astype(jnp.float32) * conv_three(product, mix_taps)).astype(jnp.bfloat16)
    full_mix_out = lax.all_gather(w_mix_out, "fs", axis=1, tiled=True)
    partial_value = jnp.dot(mixed, full_mix_out, preferred_element_type=jnp.float32)
    middle = settle(partial_value, resid, mix_post_gain)
    middle_f = middle.astype(jnp.float32)
    normed_two = norm_scale(middle_f, ffn_pre_gain).astype(jnp.bfloat16)
    full_linear, full_gated = (
        lax.all_gather(w_linear, "fs", axis=0, tiled=True),
        lax.all_gather(w_gated, "fs", axis=0, tiled=True),
    )
    linear = jnp.dot(normed_two, full_linear, preferred_element_type=jnp.float32)
    gated = jnp.dot(normed_two, full_gated, preferred_element_type=jnp.float32)
    linear = linear.astype(jnp.bfloat16)
    gated = gated.astype(jnp.bfloat16)
    activated = jax.nn.gelu(
        conv_three(gated.astype(jnp.float32), ffn_taps) + ffn_bias, approximate=True
    )
    hidden = (activated * linear.astype(jnp.float32)).astype(jnp.bfloat16)
    full_down = lax.all_gather(w_down, "fs", axis=1, tiled=True)
    partial_two = jnp.dot(hidden, full_down, preferred_element_type=jnp.float32)
    return settle(partial_two, middle_f, ffn_post_gain)


def solution(mesh):
    in_specs = (
        P(("rep", "fs"), None),
        P(),
        P("fs", "tp"),
        P("fs", "tp"),
        P("fs", "tp"),
        P(None, "tp"),
        P("tp", "fs"),
        P(),
        P(),
        P("fs", "tp"),
        P("fs", "tp"),
        P(None, "tp"),
        P("tp"),
        P("tp", "fs"),
        P(),
    )
    out_specs = P(("rep", "fs"), None)
    return jax.shard_map(
        on_device, mesh=mesh, in_specs=in_specs, out_specs=out_specs, check_vma=False
    )
```

profile of v0, /device:TPU:0, one launch (start us, length us, event | category | flops | bytes accessed | tf_op | source)
XLA Modules:
  0.0 331.4 jit_solution(645357725762932306)
XLA Ops:
  7.4 0.0 all-reduce.5.cloned.1.call-start
  7.4 1.5 fusion.8
  8.8 18.7 %all_gather.22 = bf16[1536,192]{0,1:T(8,128)(2,1)S(1)} all-gather(bf16[384,192]{0,1:T(8,128)(2,1)} %param.18), channel_id=1, replica_groups=mesh['rep'=2,'fs'=4,'tp'=4] {'fs'}, dimensions={0}, use_global_device_ids=true | all-gather | bytes 737280 | tf_op jit(solution)/shard_map/all_gather | solution.py:48
  27.5 0.0 copy-done.1
  27.5 16.1 %all_gather.23 = bf16[1536,192]{0,1:T(8,128)(2,1)S(1)} all-gather(bf16[384,192]{0,1:T(8,128)(2,1)S(1)} %copy-done.1), channel_id=1, replica_groups=mesh['rep'=2,'fs'=4,'tp'=4] {'fs'}, dimensions={0}, use_global_device_ids=true | all-gather | bytes 737280 | tf_op jit(solution)/shard_map/all_gather | solution.py:49
  43.7 0.0 copy-done
  43.7 0.0 copy-done.8
  43.7 0.5 fusion.18
  44.2 0.0 copy-start.7
  44.2 0.0 copy-start.2
  44.2 0.0 copy-start.3
  44.2 0.5 fusion.17
  44.7 0.1 reshape.58
  44.9 0.0 copy-done.7
  44.9 0.2 copy-done.2
  45.1 16.4 %all_gather.21 = bf16[1536,192]{0,1:T(8,128)(2,1)S(1)} all-gather(bf16[384,192]{0,1:T(8,128)(2,1)S(1)} %copy-done.2), channel_id=1, replica_groups=mesh['rep'=2,'fs'=4,'tp'=4] {'fs'}, dimensions={0}, use_global_device_ids=true | all-gather | bytes 737280 | tf_op jit(solution)/shard_map/all_gather | solution.py:47
  61.5 0.0 copy-done.3
  61.5 15.5 %all_gather.24 = bf16[192,1536]{1,0:T(8,128)(2,1)S(1)} all-gather(bf16[192,384]{1,0:T(8,128)(2,1)S(1)} %copy-done.3), channel_id=1, replica_groups=mesh['rep'=2,'fs'=4,'tp'=4] {'fs'}, dimensions={1}, use_global_device_ids=true | all-gather | bytes 737280 | tf_op jit(solution)/shard_map/all_gather | solution.py:59
  77.0 1.2 fusion.43
  78.2 2.1 convolution_convert_fusion.3
  80.3 0.0 all-reduce.5.cloned.1.call-update
  80.4 0.0 copy-start.5
  80.4 0.0 all-gather.4.cloned.1.call-start
  80.4 0.5 all-gather.4.cloned.1.call-update
  80.9 0.0 all-gather.6.cloned.1.call-start
  81.0 0.5 all-gather.6.cloned.1.call-update
  81.5 0.0 all-gather.8.cloned.1.call-start
  81.6 0.5 all-gather.8.cloned.1.call-update
  82.1 0.0 all-reduce.7.cloned.1.call-start
  82.2 0.0 copy-done.4
  82.2 0.0 copy-start.9
  82.2 34.8 %all-reduce.5.cloned.1.call-done = bf16[256,1536]{1,0:T(8,128)(2,1)} async-done(((bf16[256,1536]{1,0:T(8,128)(2,1)}), bf16[256,1536]{1,0:T(8,128)(2,1)}) %all-reduce.5.cloned.1.call-update) | async-done | bytes 786448 | tf_op jit(solution)/shard_map/psum | solution.py:23
  117.0 1.4 fusion.4
  118.4 1.7 fusion.12
  120.1 28.7 %all-gather.4.cloned.1.call-done = bf16[1536,1056]{0,1:T(8,128)(2,1)} async-done(((bf16[384,1056]{0,1:T(8,128)(2,1)}), bf16[1536,1056]{0,1:T(8,128)(2,1)}) %all-gather.4.cloned.1.call-update) | async-done | bytes 3244048 | tf_op jit(solution)/shard_map/all_gather | solution.py:66
  148.7 4.0 %fusion.2 = f32[256,1056]{0,1:T(8,128)} fusion(bf16[1536,1056]{0,1:T(8,128)(2,1)} %all-gather.4.cloned.1.call-done, bf16[256,1536]{1,0:T(8,128)(2,1)S(1)} %get-tuple-element.9, f32[1536]{0:T(1024)S(1)} %copy-done.9, f32[256]{0:T(256)S(1)} %add_rsqrt_fusion.1), kind=kOutput, calls=%fused_computation.4 | convolution fusion | flops 832585728 | bytes 5118976 | tf_op jit(solution)/shard_map/dot_general | solution.py:69
  152.8 1.8 reshape.64
  154.6 0.0 copy-start.10
  154.6 7.3 %fusion.31 = f32[2,128,1056]{1,0,2:T(2,128)} fusion(f32[2,128,1056]{1,0,2:T(2,128)S(1)} %reshape.64, f32[1056]{0:T(1024)S(1)} %get-tuple-element.6, f32[1056]{0:T(1024)S(1)} %get-tuple-element.7, f32[1056]{0:T(1024)S(1)} %get-tuple-element.5), kind=kLoop, calls=%fused_computation.51 | loop fusion | flops 1351680 | bytes 2175360 | tf_op jit(solution)/shard_map/add | solution.py:18
  162.0 51.6 %all-gather.6.cloned.1.call-done = bf16[1536,1056]{0,1:T(8,128)(2,1)} async-done(((bf16[384,1056]{0,1:T(8,128)(2,1)}), bf16[1536,1056]{0,1:T(8,128)(2,1)}) %all-gather.6.cloned.1.call-update) | async-done | bytes 3244048 | tf_op jit(solution)/shard_map/all_gather | solution.py:65
  213.5 64.8 %all-gather.8.cloned.1.call-done = bf16[1056,1536]{1,0:T(8,128)(2,1)} async-done(((bf16[1056,384]{1,0:T(8,128)(2,1)}), bf16[1056,1536]{1,0:T(8,128)(2,1)}) %all-gather.8.cloned.1.call-update) | async-done | bytes 3244048 | tf_op jit(solution)/shard_map/all_gather | solution.py:76
  278.3 0.0 copy-done.10
  278.3 7.9 %convolution_convert_fusion.2 = bf16[256,1536]{1,0:T(8,128)(2,1)} fusion(bf16[1056,1536]{1,0:T(8,128)(2,1)} %all-gather.8.cloned.1.call-done, bf16[1536,1056]{0,1:T(8,128)(2,1)} %all-gather.6.cloned.1.call-done, f32[132,8,2,128]{3,2,1,0:T(2,128)} %bitcast.31, f32[1056]{0:T(1024)S(1)} %copy-done.10, bf16[256,1536]{1,0:T(8,128)(2,1)S(1)} %get-tuple-element.9, ...), kind=kOutput, calls=%fused_computation.6 | convolution fusion | flops 1666424832 | bytes 9153664 | tf_op jit(solution)/shard_map/dot_general | solution.py:77
  286.3 0.0 all-reduce.7.cloned.1.call-update
  286.3 33.8 %all-reduce.7.cloned.1.call-done = bf16[256,1536]{1,0:T(8,128)(2,1)} async-done(((bf16[256,1536]{1,0:T(8,128)(2,1)}), bf16[256,1536]{1,0:T(8,128)(2,1)}) %all-reduce.7.cloned.1.call-update) | async-done | bytes 786448 | tf_op jit(solution)/shard_map/psum | solution.py:23
  320.1 1.4 fusion.6
  321.5 0.0 copy-done.6
  321.5 2.4 fusion.15
  (13 shorter events, 0.1 us)
Async XLA Ops:
  7.4 36.3 %copy-start = (bf16[256,1536]{1,0:T(8,128)(2,1)S(1)}, bf16[256,1536]{1,0:T(8,128)(2,1)}, u32[]{:S(2)}) copy-start(bf16[256,1536]{1,0:T(8,128)(2,1)} %param.15) | copy-start | bytes 2359300
  7.4 20.2 %copy-start.1 = (bf16[384,192]{0,1:T(8,128)(2,1)S(1)}, bf16[384,192]{0,1:T(8,128)(2,1)}, u32[]{:S(2)}) copy-start(bf16[384,192]{0,1:T(8,128)(2,1)} %param.19) | copy-start | bytes 442372
  7.4 36.3 %copy-start.8 = (f32[1536]{0:T(1024)S(1)}, f32[1536]{0:T(1024)}, u32[]{:S(2)}) copy-start(f32[1536]{0:T(1024)} %param.16) | copy-start | bytes 18436
  7.4 109.6 %all-reduce.5.cloned.1.call-start = ((), (), s32[]{:S(2)}) async-start(), calls=%async_computation | async-start | bytes 1572864 | tf_op jit(solution)/shard_map/psum | solution.py:23
  44.2 0.7 copy-start.7
  44.2 0.9 copy-start.2
  44.2 17.3 %copy-start.3 = (bf16[192,384]{1,0:T(8,128)(2,1)S(1)}, bf16[192,384]{1,0:T(8,128)(2,1)}, u32[]{:S(2)}) copy-start(bf16[192,384]{1,0:T(8,128)(2,1)} %param.21) | copy-start | bytes 442372
  80.3 1.8 copy-start.4
  80.4 38.0 %copy-start.5 = (f32[1536]{0:T(1024)S(1)}, f32[1536]{0:T(1024)}, u32[]{:S(2)}) copy-start(f32[1536]{0:T(1024)} %param.22) | copy-start | bytes 18436
  80.4 68.4 %all-gather.4.cloned.1.call-start = ((), (), s32[]{:S(2)}) async-start(), calls=%async_computation.1 | async-start | bytes 4055040 | tf_op jit(solution)/shard_map/all_gather | solution.py:66
  80.9 132.6 %all-gather.6.cloned.1.call-start = ((), (), s32[]{:S(2)}) async-start(), calls=%async_computation.2 | async-start | bytes 4055040 | tf_op jit(solution)/shard_map/all_gather | solution.py:65
  81.5 196.8 %all-gather.8.cloned.1.call-start = ((), (), s32[]{:S(2)}) async-start(), calls=%async_computation.3 | async-start | bytes 4055040 | tf_op jit(solution)/shard_map/all_gather | solution.py:76
  82.1 238.0 %all-reduce.7.cloned.1.call-start = ((), (), s32[]{:S(2)}) async-start(), calls=%async_computation.4 | async-start | bytes 1572864 | tf_op jit(solution)/shard_map/psum | solution.py:23
  82.2 66.5 %copy-start.9 = (f32[1536]{0:T(1024)S(1)}, f32[1536]{0:T(1024)}, u32[]{:S(2)}) copy-start(f32[1536]{0:T(1024)} %param.23) | copy-start | bytes 18436
  154.6 123.7 %copy-start.10 = (f32[1056]{0:T(1024)S(1)}, f32[1056]{0:T(1024)}, u32[]{:S(2)}) copy-start(f32[1056]{0:T(1024)} %param.27) | copy-start | bytes 12676
  286.3 35.2 %copy-start.6 = (f32[1536]{0:T(1024)S(1)}, f32[1536]{0:T(1024)}, u32[]{:S(2)}) copy-start(f32[1536]{0:T(1024)} %param.29) | copy-start | bytes 18436
Sparse Core Ops, SparseCore 0:
  80.5 36.4 all-reduce.4
  286.4 33.6 all-reduce.6
Sparse Core Ops, SparseCore 1:
  82.4 66.2 all-gather.3
  150.2 63.3 all-gather.5
  215.0 63.3 all-gather.7
where the time goes:
time: 332 us; the launch traced here: 331 us
  waiting for transfers between devices  215 us (65%)
  blocking collectives  66.7 us (20%)
  other arithmetic  16.8 us (5%)
  between operations  15.2 us (5%)
  matrix products  15.1 us (5%)
    psum x2, waiting for transfers between devices, settle(): branch = lax.psum(partial_value.astype(jnp.bfloat16), 'tp')  68.6 us
    all_gather x1, waiting for transfers between devices, on_device(): full_down = lax.all_gather(w_down, 'fs', axis=1, tiled=True)  64.8 us
    all_gather x1, waiting for transfers between devices, on_device(): lax.all_gather(w_linear, 'fs', axis=0, tiled=True)  51.6 us
    all_gather x1, waiting for transfers between devices, on_device(): lax.all_gather(w_gated, 'fs', axis=0, tiled=True)  28.7 us
    all_gather x1, blocking collectives, on_device(): lax.all_gather(w_inner_gate, 'fs', axis=0, tiled=True)  18.7 us
    all_gather x1, blocking collectives, on_device(): lax.all_gather(w_outer_gate, 'fs', axis=0, tiled=True)  16.4 us
    all_gather x1, blocking collectives, on_device(): lax.all_gather(w_value, 'fs', axis=0, tiled=True)  16.1 us
    all_gather x1, blocking collectives, on_device(): full_mix_out = lax.all_gather(w_mix_out, 'fs', axis=1, tiled=True)  15.5 us
  transfers between devices with their start and end apart: 5, of which 5 were waited for; matrix products, arithmetic and copies ran while one was open for 5% of the time, Pallas kernels for 0%

commit v1 on v0

--- a/solution.py
+++ b/solution.py
@@ -45,7 +45,9 @@
     normed = norm_scale(resid, mix_pre_gain).astype(jnp.bfloat16)
     full_outer, full_inner, full_value = (
         lax.all_gather(w_outer_gate, "fs", axis=0, tiled=True),
-        lax.all_gather(w_inner_gate, "fs", axis=0, tiled=True),
+        jnp.concatenate(
+            lax.all_to_all(jnp.stack([w_inner_gate] * lax.axis_size("fs")), "fs", 0, 0), axis=0
+        ),
         lax.all_gather(w_value, "fs", axis=0, tiled=True),
     )
     outer = jnp.dot(normed, full_outer, preferred_element_type=jnp.float32)

time: 332 us -> 332 us (level)
  blocking collectives: 66.7 us -> 60.2 us
  starting transfers between devices: 0.17 us -> 6.65 us
    all_gather x1 -> x0, blocking collectives: 18.7 us -> none  [on_device(): lax.all_gather(w_inner_gate, 'fs', axis=0, tiled=True)]
    all_gather x1, blocking collectives: 16.1 us -> 26.9 us  [on_device(): lax.all_gather(w_value, 'fs', axis=0, tiled=True)]
    all_to_all x0 -> x1, starting transfers between devices: none -> 6.48 us  [on_device(): lax.all_to_all(jnp.stack([w_inner_gate] * lax.axis_size('fs')), 'fs', 0, 0)]
  transfers between devices with their start and end apart: 5 -> 6, of which waited for: 5 -> 5; matrix products, arithmetic and copies ran while one was open for 5% -> 5% of each run, Pallas kernels for 0% -> 0%
where the time goes in v1:
time: 332 us; the launch traced here: 331 us
  waiting for transfers between devices  215 us (65%)
  blocking collectives  60.2 us (18%)
  other arithmetic  15.5 us (5%)
  between operations  15.2 us (5%)
  matrix products  15.1 us (5%)
  starting transfers between devices  6.65 us (2%)
  local copies, waits for them, and re-layouts  3.94 us (1%)
    psum x2, waiting for transfers between devices, settle(): branch = lax.psum(partial_value.astype(jnp.bfloat16), 'tp')  67.9 us
    all_gather x1, waiting for transfers between devices, on_device(): full_down = lax.all_gather(w_down, 'fs', axis=1, tiled=True)  64.8 us
    all_gather x1, waiting for transfers between devices, on_device(): lax.all_gather(w_linear, 'fs', axis=0, tiled=True)  51.6 us
    all_gather x1, waiting for transfers between devices, on_device(): lax.all_gather(w_gated, 'fs', axis=0, tiled=True)  28.7 us
    all_gather x1, blocking collectives, on_device(): lax.all_gather(w_value, 'fs', axis=0, tiled=True)  26.9 us
    all_gather x1, blocking collectives, on_device(): lax.all_gather(w_outer_gate, 'fs', axis=0, tiled=True)  18 us
    all_gather x1, blocking collectives, on_device(): full_mix_out = lax.all_gather(w_mix_out, 'fs', axis=1, tiled=True)  15.3 us
    add x2, other arithmetic, conv_three(): taps[0] * padded[:, :-2] + taps[1] * padded[:, 1:-1]  8.51 us
  transfers between devices with their start and end apart: 6, of which 5 were waited for; matrix products, arithmetic and copies ran while one was open for 5% of the time, Pallas kernels for 0%

profile of v1, /device:TPU:0, one launch (start us, length us, event | category | flops | bytes accessed | tf_op | source)
XLA Modules:
  0.0 331.2 jit_solution(16020114559799785290)
XLA Ops:
  7.4 1.9 stack.2
  9.2 6.5 %all-to-all-start = ((bf16[4,384,192]{1,2,0:T(8,128)(2,1)}), bf16[4,384,192]{1,2,0:T(8,128)(2,1)S(1)}, u32[]{:S(2)}, u32[]{:S(2)}) async-start(bf16[4,384,192]{1,2,0:T(8,128)(2,1)} %stack.2), calls=%async_computation | async-start | bytes 1179648 | tf_op jit(solution)/shard_map/all_to_all | solution.py:49
  15.7 0.0 all-reduce.5.cloned.1.call-start
  15.7 0.0 copy-done
  15.7 0.2 fusion.8
  16.0 0.0 copy-done.1
  16.0 0.0 copy-start.8
  16.0 26.9 %all_gather.19 = bf16[1536,192]{0,1:T(8,128)(2,1)S(1)} all-gather(bf16[384,192]{0,1:T(8,128)(2,1)S(1)} %copy-done.1), channel_id=1, replica_groups=mesh['rep'=2,'fs'=4,'tp'=4] {'fs'}, dimensions={0}, use_global_device_ids=true | all-gather | bytes 737280 | tf_op jit(solution)/shard_map/all_gather | solution.py:51
  42.9 0.0 copy-done.2
  42.9 18.0 %all_gather.18 = bf16[1536,192]{0,1:T(8,128)(2,1)S(1)} all-gather(bf16[384,192]{0,1:T(8,128)(2,1)S(1)} %copy-done.2), channel_id=1, replica_groups=mesh['rep'=2,'fs'=4,'tp'=4] {'fs'}, dimensions={0}, use_global_device_ids=true | all-gather | bytes 737280 | tf_op jit(solution)/shard_map/all_gather | solution.py:47
  60.9 0.0 copy-done.3
  60.9 15.3 %all_gather.20 = bf16[192,1536]{1,0:T(8,128)(2,1)S(1)} all-gather(bf16[192,384]{1,0:T(8,128)(2,1)S(1)} %copy-done.3), channel_id=1, replica_groups=mesh['rep'=2,'fs'=4,'tp'=4] {'fs'}, dimensions={1}, use_global_device_ids=true | all-gather | bytes 737280 | tf_op jit(solution)/shard_map/all_gather | solution.py:61
  76.2 0.0 copy-done.7
  76.2 0.0 all-to-all-done
  76.2 0.1 copy.18
  76.3 0.0 copy-done.8
  76.3 0.5 fusion.18
  76.8 0.5 fusion.17
  77.3 0.1 reshape.64
  77.4 1.2 fusion.43
  78.6 2.1 convolution_convert_fusion.3
  80.7 0.0 all-reduce.5.cloned.1.call-update
  80.8 0.0 copy-start.5
  80.8 0.0 all-gather.4.cloned.1.call-start
  80.8 0.5 all-gather.4.cloned.1.call-update
  81.4 0.0 all-gather.6.cloned.1.call-start
  81.4 0.5 all-gather.6.cloned.1.call-update
  81.9 0.0 all-gather.8.cloned.1.call-start
  82.0 0.5 all-gather.8.cloned.1.call-update
  82.5 0.0 all-reduce.7.cloned.1.call-start
  82.6 0.0 copy-done.4
  82.6 0.0 copy-start.9
  82.6 34.1 %all-reduce.5.cloned.1.call-done = bf16[256,1536]{1,0:T(8,128)(2,1)} async-done(((bf16[256,1536]{1,0:T(8,128)(2,1)}), bf16[256,1536]{1,0:T(8,128)(2,1)}) %all-reduce.5.cloned.1.call-update) | async-done | bytes 786448 | tf_op jit(solution)/shard_map/psum | solution.py:23
  116.8 1.4 fusion.4
  118.2 0.0 copy-done.5
  118.2 1.7 fusion.12
  119.8 28.7 %all-gather.4.cloned.1.call-done = bf16[1536,1056]{0,1:T(8,128)(2,1)} async-done(((bf16[384,1056]{0,1:T(8,128)(2,1)}), bf16[1536,1056]{0,1:T(8,128)(2,1)}) %all-gather.4.cloned.1.call-update) | async-done | bytes 3244048 | tf_op jit(solution)/shard_map/all_gather | solution.py:68
  148.5 4.0 %fusion.2 = f32[256,1056]{0,1:T(8,128)} fusion(bf16[1536,1056]{0,1:T(8,128)(2,1)} %all-gather.4.cloned.1.call-done, bf16[256,1536]{1,0:T(8,128)(2,1)S(1)} %get-tuple-element.9, f32[1536]{0:T(1024)S(1)} %copy-done.9, f32[256]{0:T(256)S(1)} %add_rsqrt_fusion.1), kind=kOutput, calls=%fused_computation.4 | convolution fusion | flops 832585728 | bytes 5118976 | tf_op jit(solution)/shard_map/dot_general | solution.py:71
  152.6 1.8 reshape.70
  154.4 0.0 copy-start.10
  154.4 7.3 %fusion.31 = f32[2,128,1056]{1,0,2:T(2,128)} fusion(f32[2,128,1056]{1,0,2:T(2,128)S(1)} %reshape.70, f32[1056]{0:T(1024)S(1)} %get-tuple-element.6, f32[1056]{0:T(1024)S(1)} %get-tuple-element.7, f32[1056]{0:T(1024)S(1)} %get-tuple-element.5), kind=kLoop, calls=%fused_computation.51 | loop fusion | flops 1351680 | bytes 2175360 | tf_op jit(solution)/shard_map/add | solution.py:18
  161.7 51.6 %all-gather.6.cloned.1.call-done = bf16[1536,1056]{0,1:T(8,128)(2,1)} async-done(((bf16[384,1056]{0,1:T(8,128)(2,1)}), bf16[1536,1056]{0,1:T(8,128)(2,1)}) %all-gather.6.cloned.1.call-update) | async-done | bytes 3244048 | tf_op jit(solution)/shard_map/all_gather | solution.py:67
  213.3 64.8 %all-gather.8.cloned.1.call-done = bf16[1056,1536]{1,0:T(8,128)(2,1)} async-done(((bf16[1056,384]{1,0:T(8,128)(2,1)}), bf16[1056,1536]{1,0:T(8,128)(2,1)}) %all-gather.8.cloned.1.call-update) | async-done | bytes 3244048 | tf_op jit(solution)/shard_map/all_gather | solution.py:78
  278.1 7.9 %convolution_convert_fusion.2 = bf16[256,1536]{1,0:T(8,128)(2,1)} fusion(bf16[1056,1536]{1,0:T(8,128)(2,1)} %all-gather.8.cloned.1.call-done, bf16[1536,1056]{0,1:T(8,128)(2,1)} %all-gather.6.cloned.1.call-done, f32[132,8,2,128]{3,2,1,0:T(2,128)} %bitcast.34, f32[1056]{0:T(1024)S(1)} %copy-done.10, bf16[256,1536]{1,0:T(8,128)(2,1)S(1)} %get-tuple-element.9, ...), kind=kOutput, calls=%fused_computation.6 | convolution fusion | flops 1666424832 | bytes 9153664 | tf_op jit(solution)/shard_map/dot_general | solution.py:79
  286.0 0.0 all-reduce.7.cloned.1.call-update
  286.1 33.8 %all-reduce.7.cloned.1.call-done = bf16[256,1536]{1,0:T(8,128)(2,1)} async-done(((bf16[256,1536]{1,0:T(8,128)(2,1)}), bf16[256,1536]{1,0:T(8,128)(2,1)}) %all-reduce.7.cloned.1.call-update) | async-done | bytes 786448 | tf_op jit(solution)/shard_map/psum | solution.py:23
  319.9 1.4 fusion.6
  321.3 2.4 fusion.15
  (16 shorter events, 0.1 us)
Async XLA Ops:
  7.4 8.4 %copy-start = (bf16[256,1536]{1,0:T(8,128)(2,1)S(1)}, bf16[256,1536]{1,0:T(8,128)(2,1)}, u32[]{:S(2)}) copy-start(bf16[256,1536]{1,0:T(8,128)(2,1)} %param.15) | copy-start | bytes 2359300
  7.4 8.6 %copy-start.1 = (bf16[384,192]{0,1:T(8,128)(2,1)S(1)}, bf16[384,192]{0,1:T(8,128)(2,1)}, u32[]{:S(2)}) copy-start(bf16[384,192]{0,1:T(8,128)(2,1)} %param.19) | copy-start | bytes 442372
  7.4 35.6 %copy-start.2 = (bf16[384,192]{0,1:T(8,128)(2,1)S(1)}, bf16[384,192]{0,1:T(8,128)(2,1)}, u32[]{:S(2)}) copy-start(bf16[384,192]{0,1:T(8,128)(2,1)} %param.17) | copy-start | bytes 442372
  9.2 51.7 %copy-start.3 = (bf16[192,384]{1,0:T(8,128)(2,1)S(1)}, bf16[192,384]{1,0:T(8,128)(2,1)}, u32[]{:S(2)}) copy-start(bf16[192,384]{1,0:T(8,128)(2,1)} %param.21) | copy-start | bytes 442372
  9.2 67.0 %all-to-all-start = ((bf16[4,384,192]{1,2,0:T(8,128)(2,1)}), bf16[4,384,192]{1,2,0:T(8,128)(2,1)S(1)}, u32[]{:S(2)}, u32[]{:S(2)}) async-start(bf16[4,384,192]{1,2,0:T(8,128)(2,1)} %stack.2), calls=%async_computation | async-start | bytes 1179648 | tf_op jit(solution)/shard_map/all_to_all | solution.py:49
  15.7 60.5 %copy-start.7 = (f32[3,192]{1,0:T(4,128)S(1)}, f32[3,192]{1,0:T(4,128)}, u32[]{:S(2)}) copy-start(f32[3,192]{1,0:T(4,128)} %param.20) | copy-start | bytes 6916
  15.7 101.1 %all-reduce.5.cloned.1.call-start = ((), (), s32[]{:S(2)}) async-start(), calls=%async_computation.1 | async-start | bytes 1572864 | tf_op jit(solution)/shard_map/psum | solution.py:23
  16.0 60.3 %copy-start.8 = (f32[1536]{0:T(1024)S(1)}, f32[1536]{0:T(1024)}, u32[]{:S(2)}) copy-start(f32[1536]{0:T(1024)} %param.16) | copy-start | bytes 18436
  80.7 1.8 copy-start.4
  80.8 37.4 %copy-start.5 = (f32[1536]{0:T(1024)S(1)}, f32[1536]{0:T(1024)}, u32[]{:S(2)}) copy-start(f32[1536]{0:T(1024)} %param.22) | copy-start | bytes 18436
  80.8 67.7 %all-gather.4.cloned.1.call-start = ((), (), s32[]{:S(2)}) async-start(), calls=%async_computation.2 | async-start | bytes 4055040 | tf_op jit(solution)/shard_map/all_gather | solution.py:68
  81.4 132.0 %all-gather.6.cloned.1.call-start = ((), (), s32[]{:S(2)}) async-start(), calls=%async_computation.3 | async-start | bytes 4055040 | tf_op jit(solution)/shard_map/all_gather | solution.py:67
  81.9 196.2 %all-gather.8.cloned.1.call-start = ((), (), s32[]{:S(2)}) async-start(), calls=%async_computation.4 | async-start | bytes 4055040 | tf_op jit(solution)/shard_map/all_gather | solution.py:78
  82.5 237.4 %all-reduce.7.cloned.1.call-start = ((), (), s32[]{:S(2)}) async-start(), calls=%async_computation.5 | async-start | bytes 1572864 | tf_op jit(solution)/shard_map/psum | solution.py:23
  82.6 65.9 %copy-start.9 = (f32[1536]{0:T(1024)S(1)}, f32[1536]{0:T(1024)}, u32[]{:S(2)}) copy-start(f32[1536]{0:T(1024)} %param.23) | copy-start | bytes 18436
  154.4 123.7 %copy-start.10 = (f32[1056]{0:T(1024)S(1)}, f32[1056]{0:T(1024)}, u32[]{:S(2)}) copy-start(f32[1056]{0:T(1024)} %param.27) | copy-start | bytes 12676
  286.0 35.2 %copy-start.6 = (f32[1536]{0:T(1024)S(1)}, f32[1536]{0:T(1024)}, u32[]{:S(2)}) copy-start(f32[1536]{0:T(1024)} %param.29) | copy-start | bytes 18436
Sparse Core Ops, SparseCore 0:
  80.9 35.8 all-reduce.4
  286.2 33.6 all-reduce.6
Sparse Core Ops, SparseCore 1:
  82.9 65.6 all-gather.3
  150.0 63.3 all-gather.5
  214.8 63.3 all-gather.7
